TPU v7x, 256 devices: a whole 4x4x8 slice. The times are simulated.
256 devices in a mesh: sp: 64 (over z, x, core), tp: 4 (over y).
Axes of the slice: x: 4, y: 4, z: 8, core: 2. Of those that a mesh axis runs over, the one named last changes fastest.
Arguments:
- moe_input: bfloat16 [16384, 2048], P('sp'), may hold values from -6 to 6
- out_cotangent: bfloat16 [16384, 2048], P('sp'), may hold values from -16 to 16
- routes: int32 [16384, 2], P('sp'), may hold values from 0 to 63, all different within a row; in each aligned block of 256 rows (0 to 255, 256 to 511, ...) at most 12 rows name the same one
- group_weight: float32 [16384], P('sp'), may hold values from 0.5 to 1
- inner_weight: float32 [16384, 2], P('sp'), may hold values from 0.3 to 1
- gate_weight: bfloat16 [64, 2048, 1024], P('sp', None, 'tp'), may hold values from -0.125 to 0.125
- up_weight: bfloat16 [64, 2048, 1024], P('sp', None, 'tp'), may hold values from -0.125 to 0.125
- down_weight: bfloat16 [64, 1024, 2048], P('sp', 'tp'), may hold values from -0.1875 to 0.1875
- value_in: bfloat16 [16384, 1024], P('sp', 'tp'), may hold values from -6 to 6
- gate_in: bfloat16 [16384, 1024], P('sp', 'tp'), may hold values from -6 to 6
- conv_taps: bfloat16 [31, 1024], P(None, 'tp'), may hold values from -1 to 1
- norm_hat: bfloat16 [16384, 1024], P('sp', 'tp'), may hold values from -6 to 6
- norm_rstd: float32 [16384], P('sp'), may hold values from 0.3 to 3
- norm_gain: float32 [1024], P('tp'), may hold values from 0.1 to 1.9
- out_proj: bfloat16 [2048, 1024], P(None, 'tp'), may hold values from -0.1875 to 0.1875
Outputs:
- gate_grad: bfloat16 [64, 2048, 1024], P('sp', None, 'tp')
- up_grad: bfloat16 [64, 2048, 1024], P('sp', None, 'tp')
- down_grad: bfloat16 [64, 1024, 2048], P('sp', 'tp')
- proj_grad: float32 [2048, 1024], P('sp', 'tp')
- value_grad: bfloat16 [16384, 1024], P('sp', 'tp')
- gate_in_grad: bfloat16 [16384, 1024], P('sp', 'tp')
Inputs may be any that keep to these rules, and one draw needn't show every extreme that they name: In the rows of one device (aligned blocks of 256 tokens) no expert is named by more than 12 routes, and in every draw some expert is named by exactly 12 in some block; a token's two experts differ.
All inputs are finite; a program needn't handle non-finite values.
Results may differ from a plain program's by a relative error of at most 0.009.
Values may be sent and summed in bfloat16 or wider, within the bound.
No kernel may reach another device: no remote copies, remote signals or barrier semaphores. Data moves between devices by JAX's collectives and lax.ppermute only.
A program may use at most 128 MiB of HBM per device.

v0:
```python
import jax
import jax.numpy as jnp
from jax import lax
from jax.sharding import PartitionSpec as P


def in_one_piece(arrays, axis, split_dim, concat_dim, along):
    ends, at = ([], 0)
    for a in arrays[:-1]:
        at += a.shape[along]
        ends.append(at)
    both = jnp.concatenate(arrays, axis=along)
    return tuple(
        jnp.split(
            lax.all_to_all(both, axis, split_axis=split_dim, concat_axis=concat_dim, tiled=True),
            ends,
            axis=along,
        )
    )


def split_up(array, dim, count):
    lengths = array.shape
    pieces = array.reshape(*lengths[:dim], count, lengths[dim] // count, *lengths[dim + 1 :])
    return jnp.moveaxis(pieces, dim, 0)


def sum_at_owner(array, axis, dim):
    count = lax.axis_size(axis)
    pieces = lax.all_to_all(split_up(array, dim, count), axis, 0, 0, tiled=True)
    return jnp.sum(pieces.astype(jnp.float32), axis=0)


def in_order(pieces, dim):
    pieces = jnp.moveaxis(pieces, 0, dim)
    lengths = pieces.shape
    return pieces.reshape(*lengths[:dim], lengths[dim] * lengths[dim + 1], *lengths[dim + 2 :])


def sent_to_all(array, axis):
    count = lax.axis_size(axis)
    return lax.all_to_all(
        jnp.broadcast_to(array[None], (count, *array.shape)), axis, 0, 0, tiled=True
    )


def gathered_copies(array, axis, dim):
    return in_order(sent_to_all(array, axis), dim)


def summed_on_arrival(array, axis, dim):
    pieces = split_up(array, dim, lax.axis_size(axis))
    arrived = lax.all_to_all(pieces, axis, split_axis=0, concat_axis=0, tiled=True)
    return arrived.sum(axis=0)


def shifted(block, axis, distance):
    devices = range(lax.axis_size(axis))
    route = [(i - distance, i) for i in devices if i - distance in devices]
    return lax.ppermute(block, axis, route)


def silu_slope(logits, squashed):
    return squashed * (1.0 + logits * (1.0 - squashed))


def on_device(
    moe_input,
    out_cotangent,
    routes,
    group_weight,
    inner_weight,
    gate_weight,
    up_weight,
    down_weight,
    value_in,
    gate_in,
    conv_taps,
    norm_hat,
    norm_rstd,
    norm_gain,
    out_proj,
):
    tok_rows, model_width = moe_input.shape
    local_experts = gate_weight.shape[0]
    sp_count = lax.axis_size("sp")
    tp_count = lax.axis_size("tp")
    all_experts = local_experts * sp_count
    capacity = 3 * tok_rows // all_experts
    col_width = model_width // tp_count
    col_start = lax.axis_index("tp") * col_width
    route_count = 2 * tok_rows
    routes_flat = routes.reshape(route_count)
    one_hot = (routes_flat[:, None] == jnp.arange(all_experts, dtype=jnp.int32)[None, :]).astype(
        jnp.int32
    )
    slot_rank = jnp.sum(one_hot * (jnp.cumsum(one_hot, axis=0) - one_hot), axis=1)
    slot_index = routes_flat * capacity + slot_rank
    slot_owner = (
        jnp.full((all_experts * capacity,), route_count, jnp.int32)
        .at[slot_index]
        .set(jnp.arange(route_count, dtype=jnp.int32))
    )
    route_weight = (group_weight[:, None] * inner_weight).reshape(route_count)
    slot_weight = jnp.concatenate([route_weight, jnp.zeros((1,), jnp.float32)])[slot_owner]
    slot_token = slot_owner // 2
    grad_cols = lax.dynamic_slice_in_dim(out_cotangent, col_start, col_width, 1)
    input_cols = lax.dynamic_slice_in_dim(moe_input, col_start, col_width, 1)
    zero_row = jnp.zeros((1, grad_cols.shape[1]), grad_cols.dtype)
    padded_grad = jnp.concatenate([grad_cols, zero_row])[slot_token]
    padded_input = jnp.concatenate([input_cols, zero_row])[slot_token]
    scaled = (slot_weight[:, None] * padded_grad.astype(jnp.float32)).astype(jnp.bfloat16)
    slot_shape = (sp_count, local_experts * capacity, grad_cols.shape[1])
    arrived = in_one_piece(
        (scaled.reshape(slot_shape), padded_input.reshape(slot_shape)), "sp", 0, 0, 1
    )
    slot_grad, slot_input = (
        lax.all_gather(arrived[0], "tp", axis=2, tiled=True),
        lax.all_gather(arrived[1], "tp", axis=2, tiled=True),
    )

    def by_expert(slot_rows):
        return (
            slot_rows.reshape(sp_count, local_experts, capacity, model_width)
            .transpose(1, 0, 2, 3)
            .reshape(local_experts, sp_count * capacity, model_width)
        )

    expert_grad = by_expert(slot_grad)
    expert_input = by_expert(slot_input)
    gate_pre = jnp.einsum(
        "emd,edf->emf", expert_input, gate_weight, preferred_element_type=jnp.float32
    )
    up_pre = jnp.einsum("emd,edf->emf", expert_input, up_weight, preferred_element_type=jnp.float32)
    gate_sigma = jax.nn.sigmoid(gate_pre)
    hidden_act = (gate_pre * gate_sigma * up_pre).astype(jnp.bfloat16)
    act_grad = jnp.einsum(
        "emd,efd->emf", expert_grad, down_weight, preferred_element_type=jnp.float32
    )
    gate_delta = (act_grad * up_pre * silu_slope(gate_pre, gate_sigma)).astype(jnp.bfloat16)
    up_delta = (act_grad * gate_pre * gate_sigma).astype(jnp.bfloat16)
    down_grad = jnp.einsum(
        "emf,emd->efd", hidden_act, expert_grad, preferred_element_type=jnp.float32
    ).astype(jnp.bfloat16)
    gate_grad = jnp.einsum(
        "emd,emf->edf", expert_input, gate_delta, preferred_element_type=jnp.float32
    ).astype(jnp.bfloat16)
    up_grad = jnp.einsum(
        "emd,emf->edf", expert_input, up_delta, preferred_element_type=jnp.float32
    ).astype(jnp.bfloat16)
    partial_value = jnp.einsum(
        "emf,edf->emd", gate_delta, gate_weight, preferred_element_type=jnp.float32
    )
    partial_value = partial_value + jnp.einsum(
        "emf,edf->emd", up_delta, up_weight, preferred_element_type=jnp.float32
    )
    summed = sum_at_owner(
        partial_value.astype(jnp.bfloat16).astype(jnp.float32).astype(jnp.bfloat16), "tp", 2
    )
    returned = summed.astype(jnp.bfloat16).reshape(local_experts, sp_count, capacity, col_width)
    returned = returned.transpose(1, 0, 2, 3).reshape(sp_count, local_experts * capacity, col_width)
    arrived_back = lax.all_to_all(returned, "sp", split_axis=0, concat_axis=0, tiled=True)
    route_grad = arrived_back.reshape(all_experts * capacity, col_width)[slot_index].astype(
        jnp.float32
    )
    mixed_cols = jnp.sum(route_grad.reshape(tok_rows, 2, col_width), axis=1)
    own_cols = lax.dynamic_slice_in_dim(out_cotangent, col_start, col_width, 1).astype(jnp.float32)
    mixer_part = (own_cols + mixed_cols).astype(jnp.bfloat16)
    mixer_grad = gathered_copies(mixer_part, "tp", 1)
    normed = norm_hat.astype(jnp.float32) * norm_gain[None, :]
    norm_sigma = jax.nn.sigmoid(normed)
    mixer_act = (normed * norm_sigma).astype(jnp.bfloat16)
    proj_grad = summed_on_arrival(
        jnp.einsum("tc,tk->ck", mixer_grad, mixer_act, preferred_element_type=jnp.float32), "sp", 0
    )
    silu_grad = jnp.dot(mixer_grad, out_proj, preferred_element_type=jnp.float32)
    hat_grad = silu_grad * silu_slope(normed, norm_sigma) * norm_gain[None, :]
    norm_values = norm_hat.astype(jnp.float32)
    grad_sum, grad_dot = lax.psum(
        (jnp.sum(hat_grad, axis=1), jnp.sum(hat_grad * norm_values, axis=1)), "tp"
    )
    channels = norm_values.shape[1] * tp_count
    conv_grad = norm_rstd[:, None] * (
        hat_grad - grad_sum[:, None] / channels - norm_values * (grad_dot[:, None] / channels)
    )
    tap_count = conv_taps.shape[0]
    incoming = shifted(conv_grad[: tap_count - 1], "sp", -1)
    extended = jnp.concatenate([conv_grad, incoming], axis=0)
    tap_values = conv_taps.astype(jnp.float32)
    glu_grad = jnp.zeros_like(conv_grad)
    for offset in range(tap_count):
        lower = tap_count - 1 - offset
        glu_grad = glu_grad + tap_values[offset][None, :] * extended[lower : lower + tok_rows]
    input_sigma = jax.nn.sigmoid(gate_in.astype(jnp.float32))
    value_grad = (glu_grad * input_sigma).astype(jnp.bfloat16)
    gate_in_grad = (
        glu_grad * value_in.astype(jnp.float32) * input_sigma * (1.0 - input_sigma)
    ).astype(jnp.bfloat16)
    return (gate_grad, up_grad, down_grad, proj_grad, value_grad, gate_in_grad)


def solution(mesh):
    return jax.shard_map(
        on_device,
        mesh=mesh,
        in_specs=(
            P("sp", None),
            P("sp", None),
            P("sp", None),
            P("sp"),
            P("sp", None),
            P("sp", None, "tp"),
            P("sp", None, "tp"),
            P("sp", "tp", None),
            P("sp", "tp"),
            P("sp", "tp"),
            P(None, "tp"),
            P("sp", "tp"),
            P("sp"),
            P("tp"),
            P(None, "tp"),
        ),
        out_specs=(
            P("sp", None, "tp"),
            P("sp", None, "tp"),
            P("sp", "tp", None),
            P("sp", "tp"),
            P("sp", "tp"),
            P("sp", "tp"),
        ),
        check_vma=False,
    )
```

profile of v0, /device:TPU:2, one launch (start us, length us, event | category | flops | bytes accessed | tf_op | source)
XLA Modules:
  0.0 374.2 jit_solution(73980024878958464)
XLA Ops:
  7.2 0.8 broadcast_multiply_fusion
  8.0 0.8 copy.30
  8.8 0.1 eq.25
  9.0 0.1 eq.29
  9.1 0.1 copy.29
  9.2 0.1 mul.444
  9.4 1.2 reduce-window.6
  10.6 0.2 slice_reduce_fusion
  10.9 0.1 fusion.120
  11.0 2.4 scatter_custom_fusion
  13.5 1.1 constant_dynamic-slice_fusion
  14.6 2.7 gather_fusion.2
  17.3 1.1 reshape.169
  18.5 3.3 gather_fusion.1
  21.8 1.2 reshape.178
  23.1 0.1 copy.28
  23.2 0.1 reshape.167
  23.4 3.2 gather_fusion
  26.6 0.1 mul.446
  26.7 0.2 multiply_convert_fusion
  26.9 1.0 copy-done.2
  27.9 0.5 pad_maximum_fusion
  28.4 51.8 %all_to_all.25 = bf16[64,24,512]{2,1,0:T(8,128)(2,1)S(1)} all-to-all(bf16[64,24,512]{2,1,0:T(8,128)(2,1)S(1)} %pad_maximum_fusion), channel_id=1, replica_groups=mesh['sp'=64,'tp'=4] {'sp'}, dimensions={0} | all-to-all | bytes 3145728 | tf_op jit(solution)/shard_map/all_to_all | solution.py:15
  80.3 1.9 fusion.132
  82.1 0.2 all-gather.5.cloned.1.call-start
  82.4 0.5 all-gather.5.cloned.1.call-update
  82.9 46.5 %all-gather.3.cloned.1.call-done = bf16[64,12,2048]{2,1,0:T(8,128)(2,1)} async-done(((bf16[64,12,512]{2,1,0:T(8,128)(2,1)}), bf16[64,12,2048]{2,1,0:T(8,128)(2,1)}) %all-gather.3.cloned.1.call-update) | async-done | bytes 3145744 | tf_op jit(solution)/shard_map/all_gather | solution.py:119
  129.4 6.2 %reshape.170 = bf16[768,2048]{1,0:T(8,128)(2,1)} reshape(bf16[64,12,2048]{2,1,0:T(8,128)(2,1)} %all-gather.3.cloned.1.call-done) | data formatting | bytes 6291456 | tf_op jit(solution)/shard_map/reshape.22
  135.6 3.9 %fusion.6 = f32[768,256]{1,0:T(8,128)} fusion(bf16[768,2048]{1,0:T(8,128)(2,1)} %reshape.170, bf16[1,2048,256]{2,1,0:T(8,128)(2,1)S(1)} %copy-done), kind=kOutput, calls=%fused_computation.48 | convolution fusion | flops 805306368 | bytes 4980736 | tf_op jit(solution)/shard_map/emd,edf->emf/dot_general | solution.py:131
  139.5 2.0 fusion.9
  141.5 41.5 %all-gather.5.cloned.1.call-done = bf16[64,12,2048]{2,1,0:T(8,128)(2,1)} async-done(((bf16[64,12,512]{2,1,0:T(8,128)(2,1)}), bf16[64,12,2048]{2,1,0:T(8,128)(2,1)}) %all-gather.5.cloned.1.call-update) | async-done | bytes 3145744 | tf_op jit(solution)/shard_map/all_gather | solution.py:118
  183.0 6.2 %reshape.171 = bf16[768,2048]{1,0:T(8,128)(2,1)} reshape(bf16[64,12,2048]{2,1,0:T(8,128)(2,1)} %all-gather.5.cloned.1.call-done) | data formatting | bytes 6291456 | tf_op jit(solution)/shard_map/reshape.3
  189.1 3.8 %multiply_convert_fusion.2 = (bf16[768,256]{1,0:T(8,128)(2,1)S(1)}, bf16[768,256]{1,0:T(8,128)(2,1)S(1)}) fusion(f32[768,256]{1,0:T(8,128)} %fusion.6, f32[768,256]{1,0:T(8,128)} %fusion.9, bf16[768,2048]{1,0:T(8,128)(2,1)} %reshape.171, bf16[1,256,2048]{2,1,0:T(8,128)(2,1)} %param.22), kind=kOutput, calls=%fused_computation.56 | convolution fusion | flops 807862272 | bytes 6553600 | tf_op jit(solution)/shard_map/emd,efd->emf/dot_general | solution.py:137
  192.9 1.0 fusion.4
  194.0 2.7 add_convert_fusion
  196.7 4.8 %reshape.175 = bf16[1,768,4,512]{3,2,1,0:T(4,128)(2,1)S(1)} reshape(bf16[768,2048]{1,0:T(8,128)(2,1)} %add_convert_fusion) | data formatting | bytes 6291456 | tf_op jit(solution)/shard_map/reshape | solution.py:24
  201.5 0.6 copy.38
  202.1 40.5 %all_to_all.26 = bf16[4,1,768,512]{3,2,1,0:T(8,128)(2,1)S(1)} all-to-all(bf16[4,1,768,512]{3,2,1,0:T(8,128)(2,1)S(1)} %bitcast.99), channel_id=1, replica_groups=mesh['sp'=64,'tp'=4] {'tp'}, dimensions={0} | all-to-all | bytes 6291456 | tf_op jit(solution)/shard_map/all_to_all | solution.py:30
  242.6 1.6 reduce_sum.61
  244.2 2.1 reshape_transpose_reshape.2
  246.3 10.5 %all-to-all-start.2 = ((bf16[64,12,512]{2,1,0:T(8,128)(2,1)}), bf16[64,12,512]{2,1,0:T(8,128)(2,1)S(1)}, u32[]{:S(2)}, u32[]{:S(2)}) async-start(bf16[64,12,512]{2,1,0:T(8,128)(2,1)} %reshape_transpose_reshape.2), calls=%async_computation.2 | async-start | bytes 2097152 | tf_op jit(solution)/shard_map/all_to_all | solution.py:162
  256.9 28.8 %all-to-all-done.2 = bf16[64,12,512]{2,1,0:T(8,128)(2,1)S(1)} async-done(((bf16[64,12,512]{2,1,0:T(8,128)(2,1)}), bf16[64,12,512]{2,1,0:T(8,128)(2,1)S(1)}, u32[]{:S(2)}, u32[]{:S(2)}) %all-to-all-start.2) | async-done | bytes 786464 | tf_op jit(solution)/shard_map/all_to_all | solution.py:162
  285.6 0.2 reshape.176
  285.8 2.0 gather_fusion.3
  287.8 0.7 reshape.179
  288.5 1.2 reduce_sum.62
  289.7 0.1 add_convert_fusion.1
  289.8 0.1 copy.34
  290.0 16.8 %all_to_all.27 = bf16[4,256,512]{1,2,0:T(8,128)(2,1)S(1)} all-to-all(bf16[4,256,512]{1,2,0:T(8,128)(2,1)S(1)} %broadcast_in_dim.11), channel_id=1, replica_groups=mesh['sp'=64,'tp'=4] {'tp'}, dimensions={0} | all-to-all | bytes 2097152 | tf_op jit(solution)/shard_map/all_to_all | solution.py:42
  306.9 1.8 fusion.116
  308.7 6.6 %all-to-all-start.4 = ((f32[64,32,256]{2,1,0:T(8,128)}), f32[64,32,256]{2,1,0:T(8,128)S(1)}, u32[]{:S(2)}, u32[]{:S(2)}) async-start(f32[64,32,256]{2,1,0:T(8,128)} %fusion.116), calls=%async_computation.4 | async-start | bytes 4194304 | tf_op jit(solution)/shard_map/all_to_all | solution.py:53
  315.4 0.6 fusion.134
  316.0 0.7 fusion.133
  316.7 4.0 %fusion = bf16[1,2048,256]{2,1,0:T(8,128)(2,1)} fusion(bf16[768,2048]{1,0:T(8,128)(2,1)} %reshape.170, bf16[768,256]{1,0:T(8,128)(2,1)S(1)} %copy-done.6), kind=kOutput, calls=%fused_computation.39 | convolution fusion | flops 805830656 | bytes 4587520 | tf_op jit(solution)/shard_map/emd,emf->edf/dot_general | solution.py:145
  320.8 2.1 fusion.2
  322.9 0.6 fusion.130
  323.5 8.9 %all-reduce.2 = (f32[256]{0:T(256)S(1)}, f32[256]{0:T(256)S(1)}) all-reduce(f32[256]{0:T(256)S(1)} %get-tuple-element.7, f32[256]{0:T(256)S(1)} %get-tuple-element.6), channel_id=1, replica_groups=mesh['sp'=64,'tp'=4] {'tp'}, use_global_device_ids=true, to_apply=%region_10.11 | all-reduce | flops 512 | bytes 4096 | tf_op jit(solution)/shard_map/psum | solution.py:179
  332.4 0.2 fusion.113
  332.9 1.9 collective-permute-start
  334.8 4.0 %fusion.1 = bf16[1,2048,256]{2,1,0:T(8,128)(2,1)} fusion(bf16[768,2048]{1,0:T(8,128)(2,1)} %reshape.170, bf16[768,256]{1,0:T(8,128)(2,1)} %copy-done.11), kind=kOutput, calls=%fused_computation.40 | convolution fusion | flops 805830656 | bytes 4587520 | tf_op jit(solution)/shard_map/emd,emf->edf/dot_general | solution.py:148
  339.2 2.1 multiply_convert_fusion.5
  341.3 0.7 multiply_convert_fusion.6
  342.0 24.6 %all-to-all-done.4 = f32[64,32,256]{2,1,0:T(8,128)S(1)} async-done(((f32[64,32,256]{2,1,0:T(8,128)}), f32[64,32,256]{2,1,0:T(8,128)S(1)}, u32[]{:S(2)}, u32[]{:S(2)}) %all-to-all-start.4) | async-done | bytes 2097184 | tf_op jit(solution)/shard_map/all_to_all | solution.py:53
  366.6 0.8 reduce_sum.63
  (124 shorter events, 0.5 us)
Async XLA Ops:
  7.2 128.4 %copy-start = (bf16[1,2048,256]{2,1,0:T(8,128)(2,1)S(1)}, bf16[1,2048,256]{2,1,0:T(8,128)(2,1)}, u32[]{:S(2)}) copy-start(bf16[1,2048,256]{2,1,0:T(8,128)(2,1)} %param.20) | copy-start | bytes 3145732
  7.2 122.2 %all-gather.3.cloned.1.call-start = ((), (), s32[]{:S(2)}) async-start(), calls=%async_computation.5 | async-start | bytes 5242880 | tf_op jit(solution)/shard_map/all_gather | solution.py:119
  18.5 4.6 %copy-start.45 = (f32[256,2]{0,1:T(2,128)S(1)}, f32[256,2]{0,1:T(2,128)}, u32[]{:S(2)}) copy-start(f32[256,2]{0,1:T(2,128)} %param.19) | copy-start | bytes 6148
  18.5 4.6 %copy-start.49 = (f32[256]{0:T(256)S(1)}, f32[256]{0:T(256)}, u32[]{:S(2)}) copy-start(f32[256]{0:T(256)} %param.18) | copy-start | bytes 3076
  26.7 1.2 copy-start.2
  82.1 100.8 %all-gather.5.cloned.1.call-start = ((), (), s32[]{:S(2)}) async-start(), calls=%async_computation.6 | async-start | bytes 5242880 | tf_op jit(solution)/shard_map/all_gather | solution.py:118
  135.6 3.9 %copy-start.3 = (bf16[768,2048]{1,0:T(8,128)(2,1)S(1)}, bf16[768,2048]{1,0:T(8,128)(2,1)}, u32[]{:S(2)}) copy-start(bf16[768,2048]{1,0:T(8,128)(2,1)} %reshape.170) | copy-start | bytes 9437188
  135.6 3.9 %copy-start.7 = (bf16[1,2048,256]{2,1,0:T(8,128)(2,1)S(1)}, bf16[1,2048,256]{2,1,0:T(8,128)(2,1)}, u32[]{:S(2)}) copy-start(bf16[1,2048,256]{2,1,0:T(8,128)(2,1)} %param.21) | copy-start | bytes 3145732
  192.9 1.0 copy-start.5
  192.9 1.0 copy-start.11
  246.3 39.3 %all-to-all-start.2 = ((bf16[64,12,512]{2,1,0:T(8,128)(2,1)}), bf16[64,12,512]{2,1,0:T(8,128)(2,1)S(1)}, u32[]{:S(2)}, u32[]{:S(2)}) async-start(bf16[64,12,512]{2,1,0:T(8,128)(2,1)} %reshape_transpose_reshape.2), calls=%async_computation.2 | async-start | bytes 2097152 | tf_op jit(solution)/shard_map/all_to_all | solution.py:162
  288.4 18.4 %copy-start.8 = (bf16[256,256]{1,0:T(8,128)(2,1)S(1)}, bf16[256,256]{1,0:T(8,128)(2,1)}, u32[]{:S(2)}) copy-start(bf16[256,256]{1,0:T(8,128)(2,1)} %param.26) | copy-start | bytes 393220
  288.5 18.4 %copy-start.46 = (f32[256]{0:T(256)S(1)}, f32[256]{0:T(256)}, u32[]{:S(2)}) copy-start(f32[256]{0:T(256)} %param.28) | copy-start | bytes 3076
  306.8 8.5 %copy-start.13 = (bf16[31,256]{1,0:T(8,128)(2,1)S(1)}, bf16[31,256]{1,0:T(8,128)(2,1)}, u32[]{:S(2)}) copy-start(bf16[31,256]{1,0:T(8,128)(2,1)} %param.25) | copy-start | bytes 47620
  306.9 9.8 %copy-start.6 = (bf16[768,256]{1,0:T(8,128)(2,1)S(1)}, bf16[768,256]{1,0:T(8,128)(2,1)}, u32[]{:S(2)}) copy-start(bf16[768,256]{1,0:T(8,128)(2,1)} %copy-done.5) | copy-start | bytes 1179652
  308.7 57.9 %all-to-all-start.4 = ((f32[64,32,256]{2,1,0:T(8,128)}), f32[64,32,256]{2,1,0:T(8,128)S(1)}, u32[]{:S(2)}, u32[]{:S(2)}) async-start(f32[64,32,256]{2,1,0:T(8,128)} %fusion.116), calls=%async_computation.4 | async-start | bytes 4194304 | tf_op jit(solution)/shard_map/all_to_all | solution.py:53
  316.7 4.1 %copy-start.4 = (bf16[768,2048]{1,0:T(8,128)(2,1)S(1)}, bf16[768,2048]{1,0:T(8,128)(2,1)}, u32[]{:S(2)}) copy-start(bf16[768,2048]{1,0:T(8,128)(2,1)} %reshape.171) | copy-start | bytes 9437188
  316.7 4.1 %copy-start.51 = (f32[768,256]{1,0:T(8,128)S(1)}, f32[768,256]{1,0:T(8,128)}, u32[]{:S(2)}) copy-start(f32[768,256]{1,0:T(8,128)} %fusion.6) | copy-start | bytes 2359300
  316.7 4.1 %copy-start.52 = (f32[768,256]{1,0:T(8,128)S(1)}, f32[768,256]{1,0:T(8,128)}, u32[]{:S(2)}) copy-start(f32[768,256]{1,0:T(8,128)} %fusion.9) | copy-start | bytes 2359300
  320.8 2.1 copy-start.9
  320.8 2.1 copy-start.47
  320.8 2.1 copy-start.50
  322.9 9.5 %copy-start.48 = (f32[256]{0:T(256)S(1)}, f32[256]{0:T(256)}, u32[]{:S(2)}) copy-start(f32[256]{0:T(256)} %param.27) | copy-start | bytes 3076
  332.6 6.3 %copy-start.10 = (bf16[256,256]{1,0:T(8,128)(2,1)S(1)}, bf16[256,256]{1,0:T(8,128)(2,1)}, u32[]{:S(2)}) copy-start(bf16[256,256]{1,0:T(8,128)(2,1)} %param.24) | copy-start | bytes 393220
  332.6 6.3 %copy-start.12 = (bf16[256,256]{1,0:T(8,128)(2,1)S(1)}, bf16[256,256]{1,0:T(8,128)(2,1)}, u32[]{:S(2)}) copy-start(bf16[256,256]{1,0:T(8,128)(2,1)} %param.23) | copy-start | bytes 393220
  332.6 6.3 %copy-start.14 = (f32[1,256]{1,0:T(1,128)S(1)}, f32[1,256]{1,0:T(1,128)}, u32[]{:S(2)}) copy-start(f32[1,256]{1,0:T(1,128)} %get-tuple-element.35) | copy-start | bytes 3076
  332.6 6.3 %copy-start.15 = (f32[1,256]{1,0:T(1,128)S(1)}, f32[1,256]{1,0:T(1,128)}, u32[]{:S(2)}) copy-start(f32[1,256]{1,0:T(1,128)} %get-tuple-element.36) | copy-start | bytes 3076
  332.6 6.3 %copy-start.16 = (f32[1,256]{1,0:T(1,128)S(1)}, f32[1,256]{1,0:T(1,128)}, u32[]{:S(2)}) copy-start(f32[1,256]{1,0:T(1,128)} %get-tuple-element.37) | copy-start | bytes 3076
  332.6 6.3 %copy-start.17 = (f32[1,256]{1,0:T(1,128)S(1)}, f32[1,256]{1,0:T(1,128)}, u32[]{:S(2)}) copy-start(f32[1,256]{1,0:T(1,128)} %get-tuple-element.38) | copy-start | bytes 3076
  332.6 6.3 %copy-start.18 = (f32[1,256]{1,0:T(1,128)S(1)}, f32[1,256]{1,0:T(1,128)}, u32[]{:S(2)}) copy-start(f32[1,256]{1,0:T(1,128)} %get-tuple-element.39) | copy-start | bytes 3076
  332.6 6.3 %copy-start.19 = (f32[1,256]{1,0:T(1,128)S(1)}, f32[1,256]{1,0:T(1,128)}, u32[]{:S(2)}) copy-start(f32[1,256]{1,0:T(1,128)} %get-tuple-element.40) | copy-start | bytes 3076
  332.7 6.3 %copy-start.20 = (f32[1,256]{1,0:T(1,128)S(1)}, f32[1,256]{1,0:T(1,128)}, u32[]{:S(2)}) copy-start(f32[1,256]{1,0:T(1,128)} %get-tuple-element.41) | copy-start | bytes 3076
  332.7 6.3 %copy-start.21 = (f32[1,256]{1,0:T(1,128)S(1)}, f32[1,256]{1,0:T(1,128)}, u32[]{:S(2)}) copy-start(f32[1,256]{1,0:T(1,128)} %get-tuple-element.42) | copy-start | bytes 3076
  332.7 6.3 %copy-start.22 = (f32[1,256]{1,0:T(1,128)S(1)}, f32[1,256]{1,0:T(1,128)}, u32[]{:S(2)}) copy-start(f32[1,256]{1,0:T(1,128)} %get-tuple-element.43) | copy-start | bytes 3076
  332.7 6.3 %copy-start.23 = (f32[1,256]{1,0:T(1,128)S(1)}, f32[1,256]{1,0:T(1,128)}, u32[]{:S(2)}) copy-start(f32[1,256]{1,0:T(1,128)} %get-tuple-element.44) | copy-start | bytes 3076
  332.7 6.3 %copy-start.24 = (f32[1,256]{1,0:T(1,128)S(1)}, f32[1,256]{1,0:T(1,128)}, u32[]{:S(2)}) copy-start(f32[1,256]{1,0:T(1,128)} %get-tuple-element.45) | copy-start | bytes 3076
  332.7 6.3 %copy-start.25 = (f32[1,256]{1,0:T(1,128)S(1)}, f32[1,256]{1,0:T(1,128)}, u32[]{:S(2)}) copy-start(f32[1,256]{1,0:T(1,128)} %get-tuple-element.46) | copy-start | bytes 3076
  332.7 6.3 %copy-start.26 = (f32[1,256]{1,0:T(1,128)S(1)}, f32[1,256]{1,0:T(1,128)}, u32[]{:S(2)}) copy-start(f32[1,256]{1,0:T(1,128)} %get-tuple-element.16) | copy-start | bytes 3076
  332.7 6.3 %copy-start.27 = (f32[1,256]{1,0:T(1,128)S(1)}, f32[1,256]{1,0:T(1,128)}, u32[]{:S(2)}) copy-start(f32[1,256]{1,0:T(1,128)} %get-tuple-element.17) | copy-start | bytes 3076
  332.7 6.3 %copy-start.28 = (f32[1,256]{1,0:T(1,128)S(1)}, f32[1,256]{1,0:T(1,128)}, u32[]{:S(2)}) copy-start(f32[1,256]{1,0:T(1,128)} %get-tuple-element.18) | copy-start | bytes 3076
  332.7 6.3 %copy-start.29 = (f32[1,256]{1,0:T(1,128)S(1)}, f32[1,256]{1,0:T(1,128)}, u32[]{:S(2)}) copy-start(f32[1,256]{1,0:T(1,128)} %get-tuple-element.19) | copy-start | bytes 3076
  332.8 6.3 %copy-start.30 = (f32[1,256]{1,0:T(1,128)S(1)}, f32[1,256]{1,0:T(1,128)}, u32[]{:S(2)}) copy-start(f32[1,256]{1,0:T(1,128)} %get-tuple-element.20) | copy-start | bytes 3076
  332.8 6.3 %copy-start.31 = (f32[1,256]{1,0:T(1,128)S(1)}, f32[1,256]{1,0:T(1,128)}, u32[]{:S(2)}) copy-start(f32[1,256]{1,0:T(1,128)} %get-tuple-element.21) | copy-start | bytes 3076
  332.8 6.3 %copy-start.32 = (f32[1,256]{1,0:T(1,128)S(1)}, f32[1,256]{1,0:T(1,128)}, u32[]{:S(2)}) copy-start(f32[1,256]{1,0:T(1,128)} %get-tuple-element.22) | copy-start | bytes 3076
  332.8 6.3 %copy-start.33 = (f32[1,256]{1,0:T(1,128)S(1)}, f32[1,256]{1,0:T(1,128)}, u32[]{:S(2)}) copy-start(f32[1,256]{1,0:T(1,128)} %get-tuple-element.23) | copy-start | bytes 3076
  332.8 6.3 %copy-start.34 = (f32[1,256]{1,0:T(1,128)S(1)}, f32[1,256]{1,0:T(1,128)}, u32[]{:S(2)}) copy-start(f32[1,256]{1,0:T(1,128)} %get-tuple-element.24) | copy-start | bytes 3076
  332.8 6.3 %copy-start.35 = (f32[1,256]{1,0:T(1,128)S(1)}, f32[1,256]{1,0:T(1,128)}, u32[]{:S(2)}) copy-start(f32[1,256]{1,0:T(1,128)} %get-tuple-element.25) | copy-start | bytes 3076
  332.8 6.3 %copy-start.36 = (f32[1,256]{1,0:T(1,128)S(1)}, f32[1,256]{1,0:T(1,128)}, u32[]{:S(2)}) copy-start(f32[1,256]{1,0:T(1,128)} %get-tuple-element.26) | copy-start | bytes 3076
  332.8 6.3 %copy-start.37 = (f32[1,256]{1,0:T(1,128)S(1)}, f32[1,256]{1,0:T(1,128)}, u32[]{:S(2)}) copy-start(f32[1,256]{1,0:T(1,128)} %get-tuple-element.27) | copy-start | bytes 3076
  332.8 6.3 %copy-start.38 = (f32[1,256]{1,0:T(1,128)S(1)}, f32[1,256]{1,0:T(1,128)}, u32[]{:S(2)}) copy-start(f32[1,256]{1,0:T(1,128)} %get-tuple-element.28) | copy-start | bytes 3076
  332.8 6.3 %copy-start.39 = (f32[1,256]{1,0:T(1,128)S(1)}, f32[1,256]{1,0:T(1,128)}, u32[]{:S(2)}) copy-start(f32[1,256]{1,0:T(1,128)} %get-tuple-element.29) | copy-start | bytes 3076
  332.9 6.3 %copy-start.40 = (f32[1,256]{1,0:T(1,128)S(1)}, f32[1,256]{1,0:T(1,128)}, u32[]{:S(2)}) copy-start(f32[1,256]{1,0:T(1,128)} %get-tuple-element.30) | copy-start | bytes 3076
  332.9 6.3 %copy-start.41 = (f32[1,256]{1,0:T(1,128)S(1)}, f32[1,256]{1,0:T(1,128)}, u32[]{:S(2)}) copy-start(f32[1,256]{1,0:T(1,128)} %get-tuple-element.31) | copy-start | bytes 3076
  332.9 6.3 %copy-start.42 = (f32[1,256]{1,0:T(1,128)S(1)}, f32[1,256]{1,0:T(1,128)}, u32[]{:S(2)}) copy-start(f32[1,256]{1,0:T(1,128)} %get-tuple-element.32) | copy-start | bytes 3076
  332.9 6.3 %copy-start.43 = (f32[1,256]{1,0:T(1,128)S(1)}, f32[1,256]{1,0:T(1,128)}, u32[]{:S(2)}) copy-start(f32[1,256]{1,0:T(1,128)} %get-tuple-element.33) | copy-start | bytes 3076
  332.9 6.3 %copy-start.44 = (f32[1,256]{1,0:T(1,128)S(1)}, f32[1,256]{1,0:T(1,128)}, u32[]{:S(2)}) copy-start(f32[1,256]{1,0:T(1,128)} %get-tuple-element.34) | copy-start | bytes 3076
  332.9 6.0 %collective-permute-start = (f32[30,256]{1,0:T(8,128)S(1)}, f32[30,256]{1,0:T(8,128)S(1)}, u32[]{:S(2)}, u32[]{:S(2)}) collective-permute-start(f32[30,256]{1,0:T(8,128)S(1)} %slice.266), channel_id=1, source_target_pairs={{4,0},{8,4},{12,8},{16,12},{20,16},{24,20},{28,24},{32,28},{36,32}... | collective-permute-start | bytes 92168 | tf_op jit(solution)/shard_map/ppermute | solution.py:60
  334.8 32.5 %copy-start.1 = (bf16[1,2048,256]{2,1,0:T(8,128)(2,1)S(1)}, bf16[1,2048,256]{2,1,0:T(8,128)(2,1)}, u32[]{:S(2)}) copy-start(bf16[1,2048,256]{2,1,0:T(8,128)(2,1)} %param.20) | copy-start | bytes 3145732
Sparse Core Ops, SparseCore 0:
  82.3 47.1 all-gather.2
  131.8 51.1 all-gather.4
where the time goes:
time: 375 us; the launch traced here: 374 us
  waiting for transfers between devices  142 us (38%)
  blocking collectives  118 us (31%)
  local copies, waits for them, and re-layouts  44.3 us (12%)
  matrix products  26 us (7%)
  starting transfers between devices  19.4 us (5%)
  between operations  15 us (4%)
  other arithmetic  9.55 us (3%)
    all_to_all x1, blocking collectives, in_one_piece(): lax.all_to_all(both, axis, split_axis=split_dim, concat_axis=concat_dim,...  51.8 us
    all_gather x1, waiting for transfers between devices, on_device(): lax.all_gather(arrived[1], 'tp', axis=2, tiled=True)  46.5 us
    all_gather x1, waiting for transfers between devices, on_device(): lax.all_gather(arrived[0], 'tp', axis=2, tiled=True)  41.5 us
    all_to_all x1, blocking collectives, sum_at_owner(): pieces = lax.all_to_all(split_up(array, dim, count), axis, 0, 0, tiled=True)  40.5 us
    all_to_all x1, waiting for transfers between devices, on_device(): lax.all_to_all(returned, 'sp', split_axis=0, concat_axis=0, tiled=True)  28.8 us
    all_to_all x1, waiting for transfers between devices, summed_on_arrival(): lax.all_to_all(pieces, axis, split_axis=0, concat_axis=0, tiled=True)  24.6 us
    all_to_all x1, blocking collectives, sent_to_all(): lax.all_to_all(jnp.broadcast_to(array[None], (count, *array.shape)), axis...  16.8 us
    another operation x3, local copies, waits for them, and re-layouts  12.3 us
  transfers between devices with their start and end apart: 5, of which 4 were waited for; matrix products, arithmetic and copies ran while one was open for 7% of the time, Pallas kernels for 0%

commit v1 on v0

--- a/solution.py
+++ b/solution.py
@@ -115,7 +115,7 @@
         (scaled.reshape(slot_shape), padded_input.reshape(slot_shape)), "sp", 0, 0, 1
     )
     slot_grad, slot_input = (
-        lax.all_gather(arrived[0], "tp", axis=2, tiled=True),
+        jnp.concatenate(lax.all_gather(arrived[0], "tp"), axis=2),
         lax.all_gather(arrived[1], "tp", axis=2, tiled=True),
     )
 

time: 375 us -> 363 us (0.968)
  waiting for transfers between devices: 142 us -> 132 us
    all_gather x1, waiting for transfers between devices: 41.5 us -> 32.9 us  [on_device(): lax.all_gather(arrived[0], 'tp')]
    another operation x3 -> x2, local copies, waits for them, and re-layouts: 12.3 us -> 6.17 us
    all_gather x0 -> x1, local copies, waits for them, and re-layouts: none -> 4.32 us  [on_device(): lax.all_gather(arrived[0], 'tp')]
  transfers between devices with their start and end apart: 5 -> 5, of which waited for: 4 -> 4; matrix products, arithmetic and copies ran while one was open for 7% -> 8% of each run, Pallas kernels for 0% -> 0%
where the time goes in v1:
time: 363 us; the launch traced here: 362 us
  waiting for transfers between devices  132 us (36%)
  blocking collectives  118 us (33%)
  local copies, waits for them, and re-layouts  45.1 us (12%)
  matrix products  23.4 us (6%)
  starting transfers between devices  19.2 us (5%)
  between operations  15.1 us (4%)
  other arithmetic  9.55 us (3%)
    all_to_all x1, blocking collectives, in_one_piece(): lax.all_to_all(both, axis, split_axis=split_dim, concat_axis=concat_dim,...  51.8 us
    all_gather x1, waiting for transfers between devices, on_device(): lax.all_gather(arrived[1], 'tp', axis=2, tiled=True)  45.7 us
    all_to_all x1, blocking collectives, sum_at_owner(): pieces = lax.all_to_all(split_up(array, dim, count), axis, 0, 0, tiled=True)  40.4 us
    all_gather x1, waiting for transfers between devices, on_device(): lax.all_gather(arrived[0], 'tp')  32.9 us
    all_to_all x1, waiting for transfers between devices, on_device(): lax.all_to_all(returned, 'sp', split_axis=0, concat_axis=0, tiled=True)  28.8 us
    all_to_all x1, waiting for transfers between devices, summed_on_arrival(): lax.all_to_all(pieces, axis, split_axis=0, concat_axis=0, tiled=True)  24.6 us
    all_to_all x1, blocking collectives, sent_to_all(): lax.all_to_all(jnp.broadcast_to(array[None], (count, *array.shape)), axis...  16.8 us
    all_to_all x1, starting transfers between devices, on_device(): lax.all_to_all(returned, 'sp', split_axis=0, concat_axis=0, tiled=True)  10.5 us
  transfers between devices with their start and end apart: 5, of which 4 were waited for; matrix products, arithmetic and copies ran while one was open for 8% of the time, Pallas kernels for 0%

profile of v1, /device:TPU:2, one launch (start us, length us, event | category | flops | bytes accessed | tf_op | source)
XLA Modules:
  0.0 362.1 jit_solution(13051979275200827349)
XLA Ops:
  7.2 0.8 broadcast_multiply_fusion
  8.0 0.8 copy.31
  8.8 0.1 eq.25
  9.0 0.1 eq.29
  9.1 0.1 copy.30
  9.2 0.1 mul.444
  9.4 1.2 reduce-window.6
  10.6 0.2 slice_reduce_fusion
  11.0 2.4 scatter_custom_fusion
  13.5 1.1 constant_dynamic-slice_fusion
  14.6 2.7 gather_fusion.2
  17.3 1.1 reshape.172
  18.5 3.3 gather_fusion.1
  21.8 1.2 reshape.182
  23.1 0.1 copy.29
  23.2 0.1 reshape.170
  23.4 3.2 gather_fusion
  26.7 0.2 multiply_convert_fusion
  26.9 1.0 copy-done.2
  27.9 0.5 pad_maximum_fusion
  28.4 51.8 %all_to_all.25 = bf16[64,24,512]{2,1,0:T(8,128)(2,1)S(1)} all-to-all(bf16[64,24,512]{2,1,0:T(8,128)(2,1)S(1)} %pad_maximum_fusion), channel_id=1, replica_groups=mesh['sp'=64,'tp'=4] {'sp'}, dimensions={0} | all-to-all | bytes 3145728 | tf_op jit(solution)/shard_map/all_to_all | solution.py:15
  80.3 1.5 fusion.132
  81.8 0.2 all-gather.6.cloned.1.call-start
  82.0 1.3 copy.34
  83.4 45.7 %all-gather.4.cloned.1.call-done = bf16[64,12,2048]{2,1,0:T(8,128)(2,1)} async-done(((bf16[64,12,512]{2,1,0:T(8,128)(2,1)}), bf16[64,12,2048]{2,1,0:T(8,128)(2,1)}) %all-gather.4.cloned.1.call-update) | async-done | bytes 3145744 | tf_op jit(solution)/shard_map/all_gather | solution.py:119
  129.1 6.2 %reshape.173 = bf16[768,2048]{1,0:T(8,128)(2,1)} reshape(bf16[64,12,2048]{2,1,0:T(8,128)(2,1)} %all-gather.4.cloned.1.call-done) | data formatting | bytes 6291456 | tf_op jit(solution)/shard_map/reshape.23
  135.3 3.9 %fusion.6 = f32[768,256]{1,0:T(8,128)} fusion(bf16[768,2048]{1,0:T(8,128)(2,1)} %reshape.173, bf16[1,2048,256]{2,1,0:T(8,128)(2,1)S(1)} %copy-done), kind=kOutput, calls=%fused_computation.48 | convolution fusion | flops 805306368 | bytes 4980736 | tf_op jit(solution)/shard_map/emd,edf->emf/dot_general | solution.py:131
  139.2 1.9 fusion.9
  141.0 32.9 %all-gather.6.cloned.1.call-done = bf16[256,12,512]{2,0,1:T(8,128)(2,1)} async-done(((bf16[64,12,512]{2,0,1:T(8,128)(2,1)}), bf16[256,12,512]{2,0,1:T(8,128)(2,1)}) %all-gather.6.cloned.1.call-update) | async-done | bytes 3145744 | tf_op jit(solution)/shard_map/all_gather | solution.py:118
  173.9 4.3 %copy.35 = bf16[4,64,12,512]{3,0,2,1:T(4,128)(2,1)S(1)} copy(bf16[4,64,12,512]{3,1,0,2:T(8,128)(2,1)} %bitcast.110) | data formatting | bytes 6291456 | tf_op jit(solution)/shard_map/all_gather | solution.py:118
  178.3 1.0 copy.39
  179.3 0.1 copy-done.51
  179.5 0.2 copy-done.53
  179.7 0.2 copy-done.55
  179.9 1.1 multiply_convert_fusion.2
  181.1 1.0 fusion.4
  182.1 2.8 add_convert_fusion
  185.0 4.8 %reshape.179 = bf16[1,768,4,512]{3,2,1,0:T(4,128)(2,1)S(1)} reshape(bf16[768,2048]{1,0:T(8,128)(2,1)} %add_convert_fusion) | data formatting | bytes 6291456 | tf_op jit(solution)/shard_map/reshape | solution.py:24
  189.8 0.6 copy.42
  190.4 40.4 %all_to_all.26 = bf16[4,1,768,512]{3,2,1,0:T(8,128)(2,1)S(1)} all-to-all(bf16[4,1,768,512]{3,2,1,0:T(8,128)(2,1)S(1)} %bitcast.105), channel_id=1, replica_groups=mesh['sp'=64,'tp'=4] {'tp'}, dimensions={0} | all-to-all | bytes 6291456 | tf_op jit(solution)/shard_map/all_to_all | solution.py:30
  230.8 1.6 reduce_sum.61
  232.3 2.1 reshape_transpose_reshape.4
  234.4 10.5 %all-to-all-start.2 = ((bf16[64,12,512]{2,1,0:T(8,128)(2,1)}), bf16[64,12,512]{2,1,0:T(8,128)(2,1)S(1)}, u32[]{:S(2)}, u32[]{:S(2)}) async-start(bf16[64,12,512]{2,1,0:T(8,128)(2,1)} %reshape_transpose_reshape.4), calls=%async_computation.2 | async-start | bytes 2097152 | tf_op jit(solution)/shard_map/all_to_all | solution.py:162
  245.0 28.8 %all-to-all-done.2 = bf16[64,12,512]{2,1,0:T(8,128)(2,1)S(1)} async-done(((bf16[64,12,512]{2,1,0:T(8,128)(2,1)}), bf16[64,12,512]{2,1,0:T(8,128)(2,1)S(1)}, u32[]{:S(2)}, u32[]{:S(2)}) %all-to-all-start.2) | async-done | bytes 786464 | tf_op jit(solution)/shard_map/all_to_all | solution.py:162
  273.7 0.2 reshape.180
  273.9 2.0 gather_fusion.3
  275.9 0.7 reshape.183
  276.6 1.2 reduce_sum.62
  278.1 16.8 %all_to_all.27 = bf16[4,256,512]{1,2,0:T(8,128)(2,1)S(1)} all-to-all(bf16[4,256,512]{1,2,0:T(8,128)(2,1)S(1)} %broadcast_in_dim.11), channel_id=1, replica_groups=mesh['sp'=64,'tp'=4] {'tp'}, dimensions={0} | all-to-all | bytes 2097152 | tf_op jit(solution)/shard_map/all_to_all | solution.py:42
  295.0 1.9 fusion.116
  296.8 6.4 %all-to-all-start.4 = ((f32[64,32,256]{2,1,0:T(8,128)}), f32[64,32,256]{2,1,0:T(8,128)S(1)}, u32[]{:S(2)}, u32[]{:S(2)}) async-start(f32[64,32,256]{2,1,0:T(8,128)} %fusion.116), calls=%async_computation.4 | async-start | bytes 4194304 | tf_op jit(solution)/shard_map/all_to_all | solution.py:53
  303.3 0.6 fusion.134
  303.9 0.7 fusion.133
  304.6 4.1 %fusion = bf16[1,2048,256]{2,1,0:T(8,128)(2,1)} fusion(bf16[768,2048]{1,0:T(8,128)(2,1)} %reshape.173, bf16[768,256]{1,0:T(8,128)(2,1)S(1)} %copy-done.7), kind=kOutput, calls=%fused_computation.39 | convolution fusion | flops 805830656 | bytes 4587520 | tf_op jit(solution)/shard_map/emd,emf->edf/dot_general | solution.py:145
  308.7 2.1 fusion.2
  310.8 0.6 fusion.130
  311.4 8.9 %all-reduce.2 = (f32[256]{0:T(256)S(1)}, f32[256]{0:T(256)S(1)}) all-reduce(f32[256]{0:T(256)S(1)} %get-tuple-element.7, f32[256]{0:T(256)S(1)} %get-tuple-element.6), channel_id=1, replica_groups=mesh['sp'=64,'tp'=4] {'tp'}, use_global_device_ids=true, to_apply=%region_10.11 | all-reduce | flops 512 | bytes 4096 | tf_op jit(solution)/shard_map/psum | solution.py:179
  320.3 0.2 fusion.113
  320.8 1.9 collective-permute-start
  322.8 4.0 %fusion.1 = bf16[1,2048,256]{2,1,0:T(8,128)(2,1)} fusion(bf16[768,2048]{1,0:T(8,128)(2,1)} %reshape.173, bf16[768,256]{1,0:T(8,128)(2,1)} %copy-done.12), kind=kOutput, calls=%fused_computation.40 | convolution fusion | flops 805830656 | bytes 4587520 | tf_op jit(solution)/shard_map/emd,emf->edf/dot_general | solution.py:148
  327.1 2.1 multiply_convert_fusion.5
  329.2 0.7 multiply_convert_fusion.6
  330.0 24.6 %all-to-all-done.4 = f32[64,32,256]{2,1,0:T(8,128)S(1)} async-done(((f32[64,32,256]{2,1,0:T(8,128)}), f32[64,32,256]{2,1,0:T(8,128)S(1)}, u32[]{:S(2)}, u32[]{:S(2)}) %all-to-all-start.4) | async-done | bytes 2097184 | tf_op jit(solution)/shard_map/all_to_all | solution.py:53
  354.5 0.8 reduce_sum.63
  (134 shorter events, 1.0 us)
Async XLA Ops:
  7.2 128.1 %copy-start = (bf16[1,2048,256]{2,1,0:T(8,128)(2,1)S(1)}, bf16[1,2048,256]{2,1,0:T(8,128)(2,1)}, u32[]{:S(2)}) copy-start(bf16[1,2048,256]{2,1,0:T(8,128)(2,1)} %param.20) | copy-start | bytes 3145732
  7.2 121.9 %all-gather.4.cloned.1.call-start = ((), (), s32[]{:S(2)}) async-start(), calls=%async_computation.5 | async-start | bytes 5242880 | tf_op jit(solution)/shard_map/all_gather | solution.py:119
  18.5 4.6 %copy-start.46 = (f32[256,2]{0,1:T(2,128)S(1)}, f32[256,2]{0,1:T(2,128)}, u32[]{:S(2)}) copy-start(f32[256,2]{0,1:T(2,128)} %param.19) | copy-start | bytes 6148
  18.5 4.6 %copy-start.50 = (f32[256]{0:T(256)S(1)}, f32[256]{0:T(256)}, u32[]{:S(2)}) copy-start(f32[256]{0:T(256)} %param.18) | copy-start | bytes 3076
  26.7 1.2 copy-start.2
  81.8 92.1 %all-gather.6.cloned.1.call-start = ((), (), s32[]{:S(2)}) async-start(), calls=%async_computation.6 | async-start | bytes 3932160 | tf_op jit(solution)/shard_map/all_gather | solution.py:118
  135.3 3.9 %copy-start.3 = (bf16[768,2048]{1,0:T(8,128)(2,1)S(1)}, bf16[768,2048]{1,0:T(8,128)(2,1)}, u32[]{:S(2)}) copy-start(bf16[768,2048]{1,0:T(8,128)(2,1)} %reshape.173) | copy-start | bytes 9437188
  135.3 3.9 %copy-start.8 = (bf16[1,2048,256]{2,1,0:T(8,128)(2,1)S(1)}, bf16[1,2048,256]{2,1,0:T(8,128)(2,1)}, u32[]{:S(2)}) copy-start(bf16[1,2048,256]{2,1,0:T(8,128)(2,1)} %param.21) | copy-start | bytes 3145732
  178.2 1.2 copy-start.51
  178.2 1.4 copy-start.53
  178.3 1.7 copy-start.55
  179.3 1.8 copy-start.4
  181.1 1.0 copy-start.6
  181.1 1.0 copy-start.12
  234.4 39.3 %all-to-all-start.2 = ((bf16[64,12,512]{2,1,0:T(8,128)(2,1)}), bf16[64,12,512]{2,1,0:T(8,128)(2,1)S(1)}, u32[]{:S(2)}, u32[]{:S(2)}) async-start(bf16[64,12,512]{2,1,0:T(8,128)(2,1)} %reshape_transpose_reshape.4), calls=%async_computation.2 | async-start | bytes 2097152 | tf_op jit(solution)/shard_map/all_to_all | solution.py:162
  276.6 18.4 %copy-start.9 = (bf16[256,256]{1,0:T(8,128)(2,1)S(1)}, bf16[256,256]{1,0:T(8,128)(2,1)}, u32[]{:S(2)}) copy-start(bf16[256,256]{1,0:T(8,128)(2,1)} %param.26) | copy-start | bytes 393220
  276.6 18.4 %copy-start.47 = (f32[256]{0:T(256)S(1)}, f32[256]{0:T(256)}, u32[]{:S(2)}) copy-start(f32[256]{0:T(256)} %param.28) | copy-start | bytes 3076
  295.0 8.3 %copy-start.14 = (bf16[31,256]{1,0:T(8,128)(2,1)S(1)}, bf16[31,256]{1,0:T(8,128)(2,1)}, u32[]{:S(2)}) copy-start(bf16[31,256]{1,0:T(8,128)(2,1)} %param.25) | copy-start | bytes 47620
  295.0 9.6 %copy-start.7 = (bf16[768,256]{1,0:T(8,128)(2,1)S(1)}, bf16[768,256]{1,0:T(8,128)(2,1)}, u32[]{:S(2)}) copy-start(bf16[768,256]{1,0:T(8,128)(2,1)} %copy-done.6) | copy-start | bytes 1179652
  296.8 57.7 %all-to-all-start.4 = ((f32[64,32,256]{2,1,0:T(8,128)}), f32[64,32,256]{2,1,0:T(8,128)S(1)}, u32[]{:S(2)}, u32[]{:S(2)}) async-start(f32[64,32,256]{2,1,0:T(8,128)} %fusion.116), calls=%async_computation.4 | async-start | bytes 4194304 | tf_op jit(solution)/shard_map/all_to_all | solution.py:53
  304.6 4.1 %copy-start.5 = (bf16[96,8,4,512]{3,1,2,0:T(8,128)(2,1)S(1)}, bf16[96,8,4,512]{3,1,2,0:T(8,128)(2,1)}, u32[]{:S(2)}) copy-start(bf16[96,8,4,512]{3,1,2,0:T(8,128)(2,1)} %copy-done.4) | copy-start | bytes 9437188
  304.6 4.1 %copy-start.54 = (f32[768,256]{1,0:T(8,128)S(1)}, f32[768,256]{1,0:T(8,128)}, u32[]{:S(2)}) copy-start(f32[768,256]{1,0:T(8,128)} %fusion.6) | copy-start | bytes 2359300
  304.6 4.1 %copy-start.56 = (f32[768,256]{1,0:T(8,128)S(1)}, f32[768,256]{1,0:T(8,128)}, u32[]{:S(2)}) copy-start(f32[768,256]{1,0:T(8,128)} %fusion.9) | copy-start | bytes 2359300
  308.7 2.1 copy-start.10
  308.7 2.1 copy-start.48
  308.7 2.1 copy-start.52
  310.8 9.5 %copy-start.49 = (f32[256]{0:T(256)S(1)}, f32[256]{0:T(256)}, u32[]{:S(2)}) copy-start(f32[256]{0:T(256)} %param.27) | copy-start | bytes 3076
  320.5 6.3 %copy-start.11 = (bf16[256,256]{1,0:T(8,128)(2,1)S(1)}, bf16[256,256]{1,0:T(8,128)(2,1)}, u32[]{:S(2)}) copy-start(bf16[256,256]{1,0:T(8,128)(2,1)} %param.24) | copy-start | bytes 393220
  320.5 6.3 %copy-start.13 = (bf16[256,256]{1,0:T(8,128)(2,1)S(1)}, bf16[256,256]{1,0:T(8,128)(2,1)}, u32[]{:S(2)}) copy-start(bf16[256,256]{1,0:T(8,128)(2,1)} %param.23) | copy-start | bytes 393220
  320.5 6.3 %copy-start.15 = (f32[1,256]{1,0:T(1,128)S(1)}, f32[1,256]{1,0:T(1,128)}, u32[]{:S(2)}) copy-start(f32[1,256]{1,0:T(1,128)} %get-tuple-element.35) | copy-start | bytes 3076
  320.5 6.3 %copy-start.16 = (f32[1,256]{1,0:T(1,128)S(1)}, f32[1,256]{1,0:T(1,128)}, u32[]{:S(2)}) copy-start(f32[1,256]{1,0:T(1,128)} %get-tuple-element.36) | copy-start | bytes 3076
  320.5 6.3 %copy-start.17 = (f32[1,256]{1,0:T(1,128)S(1)}, f32[1,256]{1,0:T(1,128)}, u32[]{:S(2)}) copy-start(f32[1,256]{1,0:T(1,128)} %get-tuple-element.37) | copy-start | bytes 3076
  320.6 6.3 %copy-start.18 = (f32[1,256]{1,0:T(1,128)S(1)}, f32[1,256]{1,0:T(1,128)}, u32[]{:S(2)}) copy-start(f32[1,256]{1,0:T(1,128)} %get-tuple-element.38) | copy-start | bytes 3076
  320.6 6.3 %copy-start.19 = (f32[1,256]{1,0:T(1,128)S(1)}, f32[1,256]{1,0:T(1,128)}, u32[]{:S(2)}) copy-start(f32[1,256]{1,0:T(1,128)} %get-tuple-element.39) | copy-start | bytes 3076
  320.6 6.3 %copy-start.20 = (f32[1,256]{1,0:T(1,128)S(1)}, f32[1,256]{1,0:T(1,128)}, u32[]{:S(2)}) copy-start(f32[1,256]{1,0:T(1,128)} %get-tuple-element.40) | copy-start | bytes 3076
  320.6 6.3 %copy-start.21 = (f32[1,256]{1,0:T(1,128)S(1)}, f32[1,256]{1,0:T(1,128)}, u32[]{:S(2)}) copy-start(f32[1,256]{1,0:T(1,128)} %get-tuple-element.41) | copy-start | bytes 3076
  320.6 6.3 %copy-start.22 = (f32[1,256]{1,0:T(1,128)S(1)}, f32[1,256]{1,0:T(1,128)}, u32[]{:S(2)}) copy-start(f32[1,256]{1,0:T(1,128)} %get-tuple-element.42) | copy-start | bytes 3076
  320.6 6.3 %copy-start.23 = (f32[1,256]{1,0:T(1,128)S(1)}, f32[1,256]{1,0:T(1,128)}, u32[]{:S(2)}) copy-start(f32[1,256]{1,0:T(1,128)} %get-tuple-element.43) | copy-start | bytes 3076
  320.6 6.3 %copy-start.24 = (f32[1,256]{1,0:T(1,128)S(1)}, f32[1,256]{1,0:T(1,128)}, u32[]{:S(2)}) copy-start(f32[1,256]{1,0:T(1,128)} %get-tuple-element.44) | copy-start | bytes 3076
  320.6 6.3 %copy-start.25 = (f32[1,256]{1,0:T(1,128)S(1)}, f32[1,256]{1,0:T(1,128)}, u32[]{:S(2)}) copy-start(f32[1,256]{1,0:T(1,128)} %get-tuple-element.45) | copy-start | bytes 3076
  320.6 6.3 %copy-start.26 = (f32[1,256]{1,0:T(1,128)S(1)}, f32[1,256]{1,0:T(1,128)}, u32[]{:S(2)}) copy-start(f32[1,256]{1,0:T(1,128)} %get-tuple-element.46) | copy-start | bytes 3076
  320.6 6.3 %copy-start.27 = (f32[1,256]{1,0:T(1,128)S(1)}, f32[1,256]{1,0:T(1,128)}, u32[]{:S(2)}) copy-start(f32[1,256]{1,0:T(1,128)} %get-tuple-element.16) | copy-start | bytes 3076
  320.7 6.3 %copy-start.28 = (f32[1,256]{1,0:T(1,128)S(1)}, f32[1,256]{1,0:T(1,128)}, u32[]{:S(2)}) copy-start(f32[1,256]{1,0:T(1,128)} %get-tuple-element.17) | copy-start | bytes 3076
  320.7 6.3 %copy-start.29 = (f32[1,256]{1,0:T(1,128)S(1)}, f32[1,256]{1,0:T(1,128)}, u32[]{:S(2)}) copy-start(f32[1,256]{1,0:T(1,128)} %get-tuple-element.18) | copy-start | bytes 3076
  320.7 6.3 %copy-start.30 = (f32[1,256]{1,0:T(1,128)S(1)}, f32[1,256]{1,0:T(1,128)}, u32[]{:S(2)}) copy-start(f32[1,256]{1,0:T(1,128)} %get-tuple-element.19) | copy-start | bytes 3076
  320.7 6.3 %copy-start.31 = (f32[1,256]{1,0:T(1,128)S(1)}, f32[1,256]{1,0:T(1,128)}, u32[]{:S(2)}) copy-start(f32[1,256]{1,0:T(1,128)} %get-tuple-element.20) | copy-start | bytes 3076
  320.7 6.3 %copy-start.32 = (f32[1,256]{1,0:T(1,128)S(1)}, f32[1,256]{1,0:T(1,128)}, u32[]{:S(2)}) copy-start(f32[1,256]{1,0:T(1,128)} %get-tuple-element.21) | copy-start | bytes 3076
  320.7 6.3 %copy-start.33 = (f32[1,256]{1,0:T(1,128)S(1)}, f32[1,256]{1,0:T(1,128)}, u32[]{:S(2)}) copy-start(f32[1,256]{1,0:T(1,128)} %get-tuple-element.22) | copy-start | bytes 3076
  320.7 6.3 %copy-start.34 = (f32[1,256]{1,0:T(1,128)S(1)}, f32[1,256]{1,0:T(1,128)}, u32[]{:S(2)}) copy-start(f32[1,256]{1,0:T(1,128)} %get-tuple-element.23) | copy-start | bytes 3076
  320.7 6.3 %copy-start.35 = (f32[1,256]{1,0:T(1,128)S(1)}, f32[1,256]{1,0:T(1,128)}, u32[]{:S(2)}) copy-start(f32[1,256]{1,0:T(1,128)} %get-tuple-element.24) | copy-start | bytes 3076
  320.7 6.3 %copy-start.36 = (f32[1,256]{1,0:T(1,128)S(1)}, f32[1,256]{1,0:T(1,128)}, u32[]{:S(2)}) copy-start(f32[1,256]{1,0:T(1,128)} %get-tuple-element.25) | copy-start | bytes 3076
  320.7 6.3 %copy-start.37 = (f32[1,256]{1,0:T(1,128)S(1)}, f32[1,256]{1,0:T(1,128)}, u32[]{:S(2)}) copy-start(f32[1,256]{1,0:T(1,128)} %get-tuple-element.26) | copy-start | bytes 3076
  320.8 6.3 %copy-start.38 = (f32[1,256]{1,0:T(1,128)S(1)}, f32[1,256]{1,0:T(1,128)}, u32[]{:S(2)}) copy-start(f32[1,256]{1,0:T(1,128)} %get-tuple-element.27) | copy-start | bytes 3076
  320.8 6.3 %copy-start.39 = (f32[1,256]{1,0:T(1,128)S(1)}, f32[1,256]{1,0:T(1,128)}, u32[]{:S(2)}) copy-start(f32[1,256]{1,0:T(1,128)} %get-tuple-element.28) | copy-start | bytes 3076
  320.8 6.3 %copy-start.40 = (f32[1,256]{1,0:T(1,128)S(1)}, f32[1,256]{1,0:T(1,128)}, u32[]{:S(2)}) copy-start(f32[1,256]{1,0:T(1,128)} %get-tuple-element.29) | copy-start | bytes 3076
  320.8 6.3 %copy-start.41 = (f32[1,256]{1,0:T(1,128)S(1)}, f32[1,256]{1,0:T(1,128)}, u32[]{:S(2)}) copy-start(f32[1,256]{1,0:T(1,128)} %get-tuple-element.30) | copy-start | bytes 3076
  320.8 6.3 %copy-start.42 = (f32[1,256]{1,0:T(1,128)S(1)}, f32[1,256]{1,0:T(1,128)}, u32[]{:S(2)}) copy-start(f32[1,256]{1,0:T(1,128)} %get-tuple-element.31) | copy-start | bytes 3076
  320.8 6.3 %copy-start.43 = (f32[1,256]{1,0:T(1,128)S(1)}, f32[1,256]{1,0:T(1,128)}, u32[]{:S(2)}) copy-start(f32[1,256]{1,0:T(1,128)} %get-tuple-element.32) | copy-start | bytes 3076
  320.8 6.3 %copy-start.44 = (f32[1,256]{1,0:T(1,128)S(1)}, f32[1,256]{1,0:T(1,128)}, u32[]{:S(2)}) copy-start(f32[1,256]{1,0:T(1,128)} %get-tuple-element.33) | copy-start | bytes 3076
  320.8 6.3 %copy-start.45 = (f32[1,256]{1,0:T(1,128)S(1)}, f32[1,256]{1,0:T(1,128)}, u32[]{:S(2)}) copy-start(f32[1,256]{1,0:T(1,128)} %get-tuple-element.34) | copy-start | bytes 3076
  320.8 6.0 %collective-permute-start = (f32[30,256]{1,0:T(8,128)S(1)}, f32[30,256]{1,0:T(8,128)S(1)}, u32[]{:S(2)}, u32[]{:S(2)}) collective-permute-start(f32[30,256]{1,0:T(8,128)S(1)} %slice.266), channel_id=1, source_target_pairs={{4,0},{8,4},{12,8},{16,12},{20,16},{24,20},{28,24},{32,28},{36,32}... | collective-permute-start | bytes 92168 | tf_op jit(solution)/shard_map/ppermute | solution.py:60
  322.8 32.5 %copy-start.1 = (bf16[1,2048,256]{2,1,0:T(8,128)(2,1)S(1)}, bf16[1,2048,256]{2,1,0:T(8,128)(2,1)}, u32[]{:S(2)}) copy-start(bf16[1,2048,256]{2,1,0:T(8,128)(2,1)} %param.20) | copy-start | bytes 3145732
Sparse Core Ops, SparseCore 0:
  81.9 47.1 all-gather.3
  131.5 42.3 all-gather.5
